TPU v7x, 32 devices: a whole 2x2x4 slice. The times are simulated.
32 devices in a mesh: grp: 2 (over y), sp: 4 (over z), tp: 4 (over x, core).
Axes of the slice: x: 2, y: 2, z: 4, core: 2. Of those that a mesh axis runs over, the one named last changes fastest.
Arguments:
- tokens: bfloat16 [3072, 2048], P(('grp', 'sp'), 'tp'), parts along dimension 0, may hold values from -6 to 6
- norm_gain: float32 [2048], replicated, may hold values from 0.1 to 1.9
- qk_gain: float32 [4, 64], replicated, may hold values from 0.7 to 5.5
- w_query_window: bfloat16 [2048, 1024], P('sp', 'tp'), may hold values from -1 to 1
- w_key_window: bfloat16 [2048, 512], P('sp', 'tp'), may hold values from -1 to 1
- w_value_window: bfloat16 [2048, 512], P('sp', 'tp'), may hold values from -0.125 to 0.125
- sink_logits: float32 [16], P('tp'), may hold values from 0 to 5
- w_query_forget: bfloat16 [2048, 1024], P('sp', 'tp'), may hold values from -1 to 1
- w_key_forget: bfloat16 [2048, 1024], P('sp', 'tp'), may hold values from -1 to 1
- w_value_forget: bfloat16 [2048, 1024], P('sp', 'tp'), may hold values from -0.125 to 0.125
- gate_cum: float32 [3072, 16], P(('grp', 'sp'), 'tp'), parts along dimension 0, as said below
- w_merge: bfloat16 [2048, 2, 2048], P('sp', None, 'tp'), may hold values from -0.125 to 0.125
- w_branch: bfloat16 [2, 1024, 2048], P(None, 'sp', 'tp'), may hold values from -0.8984375 to 0.8984375
Outputs:
- mixed: bfloat16 [3072, 2048], P(('grp', 'sp'), 'tp'), parts along dimension 0
There are 2 independent parts, one for each index of `grp`. A program takes and returns all parts, laid end to end along the dimension named above; an argument that names none is the same for every part. Nothing has to cross between parts.
Inputs may be any that keep to these rules, and one draw needn't show every extreme that they name: `gate_cum`: along positions each head's values never rise.
All inputs are finite; a program needn't handle non-finite values.
Results may differ from a plain program's by a relative error of at most 0.012.
Values may be sent and summed in bfloat16 or wider, within the bound.
A program may use at most 64 MiB of HBM per device.

v0:
```python
import math
import jax
import jax.numpy as jnp
from jax import lax
from jax.sharding import PartitionSpec as P

HEAD = 64
WINDOW = 128
epsilon = 1e-06
big_negative = -1e30


def from_behind(value, axis, by):
    size = lax.axis_size(axis)
    pairs = [(i, i + by) for i in range(size) if 0 <= i + by < size]
    return lax.ppermute(value, axis, pairs)


def head_norm(raw, gain, head_count):
    split = raw.reshape(raw.shape[0], head_count, -1)
    scaled = split * lax.rsqrt(jnp.mean(split * split, axis=-1, keepdims=True) + epsilon) * gain
    return scaled.astype(jnp.bfloat16)


def window_attend(queries, keys_ext, values_ext, sink_rows, first_pos):
    row_count, head_count, head_size = queries.shape
    group_count = keys_ext.shape[1]
    span_rows = WINDOW // 2
    block_count = row_count // span_rows
    query_blocks = queries.reshape(
        block_count, span_rows, group_count, head_count // group_count, head_size
    )
    key_blocks = jnp.concatenate(
        [
            keys_ext[lag_index * span_rows : lag_index * span_rows + row_count].reshape(
                block_count, span_rows, group_count, head_size
            )
            for lag_index in range(3)
        ],
        axis=1,
    )
    value_blocks = jnp.concatenate(
        [
            values_ext[lag_index * span_rows : lag_index * span_rows + row_count].reshape(
                block_count, span_rows, group_count, head_size
            )
            for lag_index in range(3)
        ],
        axis=1,
    )
    scores = jnp.einsum(
        "nqgrd,nkgd->ngrqk", query_blocks, key_blocks, preferred_element_type=jnp.float32
    ) * head_size ** (-0.5)
    distance = WINDOW + jnp.arange(span_rows)[:, None] - jnp.arange(3 * span_rows)[None, :]
    key_pos = (
        first_pos
        - WINDOW
        + jnp.arange(block_count)[:, None] * span_rows
        + jnp.arange(3 * span_rows)[None, :]
    )
    is_valid = ((distance >= 0) & (distance < WINDOW))[None] & (key_pos >= 0)[:, None, :]
    is_valid = is_valid[:, None, None]
    sink_grid = sink_rows.reshape(1, group_count, head_count // group_count, 1)
    row_max = jnp.maximum(jnp.max(jnp.where(is_valid, scores, big_negative), axis=-1), sink_grid)
    weights = jnp.where(is_valid, jnp.exp(scores - row_max[..., None]), 0.0)
    row_total = jnp.sum(weights, axis=-1) + jnp.exp(sink_grid - row_max)
    prob_rows = (weights / row_total[..., None]).astype(jnp.bfloat16)
    mixed_sum = jnp.einsum(
        "ngrqk,nkgd->nqgrd", prob_rows, value_blocks, preferred_element_type=jnp.float32
    )
    return mixed_sum.reshape(row_count, head_count * head_size).astype(jnp.bfloat16)


def forget_groups(groups, keys, values, gates):
    head_count, head_size = (keys.shape[1], keys.shape[2])
    gates_all = lax.all_gather(gates, "sp", axis=0, tiled=True)

    def absorber(queries, query_gate, query_pos):

        def absorb(running, block):
            row_max, row_total, mixed_sum = running
            key_rows, value_rows, key_gate, key_pos = block
            scores = jnp.einsum(
                "qhd,khd->hqk", queries, key_rows, preferred_element_type=jnp.float32
            ) * head_size ** (-0.5)
            scores = scores + query_gate.T[:, :, None] - key_gate.T[:, None, :]
            is_valid = (query_pos[:, None] >= key_pos[None, :])[None]
            new_max = jnp.maximum(
                row_max, jnp.max(jnp.where(is_valid, scores, big_negative), axis=-1)
            )
            weights = jnp.where(is_valid, jnp.exp(scores - new_max[..., None]), 0.0)
            shrink = jnp.exp(row_max - new_max)
            row_total = row_total * shrink + jnp.sum(weights, axis=-1)
            mixed_sum = mixed_sum * shrink.T[:, :, None] + jnp.einsum(
                "hqk,khd->qhd",
                weights.astype(jnp.bfloat16),
                value_rows,
                preferred_element_type=jnp.float32,
            )
            return ((new_max, row_total, mixed_sum), None)

        return absorb

    initial = tuple(
        (
            (
                jnp.full((head_count, group[0].shape[0]), big_negative, jnp.float32),
                jnp.zeros((head_count, group[0].shape[0]), jnp.float32),
                jnp.zeros((group[0].shape[0], head_count, head_size), jnp.float32),
            )
            for group in groups
        )
    )
    first_row = jnp.int32(0)
    key_rows = lax.all_gather(keys, "sp", axis=0, tiled=True)
    value_rows = lax.all_gather(values, "sp", axis=0, tiled=True)
    piece_rows = key_rows.shape[0]
    sub_rows = math.gcd(piece_rows, 2048)
    turns = piece_rows // sub_rows
    key_gate = gates_all
    key_pos = jnp.arange(piece_rows)
    blocks = (
        key_rows.reshape(turns, sub_rows, head_count, head_size),
        value_rows.reshape(turns, sub_rows, head_count, head_size),
        key_gate.reshape(turns, sub_rows, head_count),
        key_pos.reshape(turns, sub_rows),
    )
    updated = []
    for (queries, query_gate, query_pos), state in zip(groups, initial):
        absorb = absorber(queries, query_gate, query_pos)

        def advance(current):
            return lax.scan(absorb, current, blocks)[0]

        def keep(current):
            return current

        updated.append(lax.cond(first_row <= query_pos[-1], advance, keep, state))
    finals = tuple(updated)
    return [
        (mixed_sum / row_total.T[:, :, None])
        .reshape(mixed_sum.shape[0], head_count * head_size)
        .astype(jnp.bfloat16)
        for row_max, row_total, mixed_sum in finals
    ]


def on_device(
    tokens,
    norm_gain,
    qk_gain,
    w_query_window,
    w_key_window,
    w_value_window,
    sink_logits,
    w_query_forget,
    w_key_forget,
    w_value_forget,
    gate_cum,
    w_merge,
    w_branch,
):
    row_count = tokens.shape[0]
    row_offset = lax.axis_index("sp") * row_count
    gathered = lax.all_gather(tokens, "tp", axis=1, tiled=True)
    as_float = gathered.astype(jnp.float32)
    normed = (
        as_float
        * lax.rsqrt(jnp.mean(as_float * as_float, axis=-1, keepdims=True) + epsilon)
        * norm_gain
    ).astype(jnp.bfloat16)
    merge_flat = w_merge.reshape(w_merge.shape[0], -1)
    pieces = (
        lax.all_gather(w_query_window, "sp", axis=0, tiled=True),
        lax.all_gather(w_key_window, "sp", axis=0, tiled=True),
        lax.all_gather(w_value_window, "sp", axis=0, tiled=True),
        lax.all_gather(w_query_forget, "sp", axis=0, tiled=True),
        lax.all_gather(w_key_forget, "sp", axis=0, tiled=True),
        lax.all_gather(w_value_forget, "sp", axis=0, tiled=True),
        lax.all_gather(merge_flat, "sp", axis=0, tiled=True),
    )
    projected = tuple(
        (jnp.dot(normed, weight_rows, preferred_element_type=jnp.float32) for weight_rows in pieces)
    )
    query_heads = w_query_window.shape[1] // HEAD
    group_heads = w_key_window.shape[1] // HEAD
    window_query = head_norm(projected[0], qk_gain[0], query_heads)
    window_key = head_norm(projected[1], qk_gain[1], group_heads)
    window_value = projected[2].astype(jnp.bfloat16).reshape(row_count, group_heads, HEAD)
    prev_key, prev_value = from_behind(
        (window_key[row_count - WINDOW :], window_value[row_count - WINDOW :]), "sp", 1
    )
    window_out = window_attend(
        window_query,
        jnp.concatenate([prev_key, window_key], axis=0),
        jnp.concatenate([prev_value, window_value], axis=0),
        sink_logits,
        row_offset,
    )
    forget_query = head_norm(projected[3], qk_gain[2], query_heads)
    forget_key = head_norm(projected[4], qk_gain[3], query_heads)
    forget_value = projected[5].astype(jnp.bfloat16).reshape(row_count, query_heads, HEAD)
    own_pos = row_offset + jnp.arange(row_count)
    forget_out = forget_groups(
        [(forget_query, gate_cum, own_pos)], forget_key, forget_value, gate_cum
    )[0]
    channel_count = w_merge.shape[2]
    merge_gate = jax.nn.sigmoid(projected[6]).reshape(row_count, 2, channel_count)
    branch_full = lax.all_gather(w_branch, "sp", axis=1, tiled=True)
    head_stack = jnp.stack([window_out, forget_out], axis=1)
    weight_rows = branch_full
    projection = jnp.einsum(
        "uxa,xag->uxg",
        lax.all_gather(head_stack, "tp", axis=2, tiled=True),
        weight_rows,
        preferred_element_type=jnp.float32,
    )
    return (merge_gate[:, 0] * projection[:, 0] + merge_gate[:, 1] * projection[:, 1]).astype(
        jnp.bfloat16
    )


def solution(mesh):
    return jax.shard_map(
        on_device,
        mesh=mesh,
        in_specs=(
            P(("grp", "sp"), "tp"),
            P(),
            P(),
            P("sp", "tp"),
            P("sp", "tp"),
            P("sp", "tp"),
            P("tp"),
            P("sp", "tp"),
            P("sp", "tp"),
            P("sp", "tp"),
            P(("grp", "sp"), "tp"),
            P("sp", None, "tp"),
            P(None, "sp", "tp"),
        ),
        out_specs=P(("grp", "sp"), "tp"),
        check_vma=False,
    )
```

profile of v0, /device:TPU:0, one launch (start us, length us, event | category | flops | bytes accessed | tf_op | source)
XLA Modules:
  0.0 339.6 jit_solution(14842164746860835694)
XLA Ops:
  13.7 16.6 %all_gather.48 = f32[1536,4]{0,1:T(4,128)} all-gather(f32[384,4]{0,1:T(4,128)} %param.27), channel_id=1, replica_groups=mesh['grp'=2,'sp'=4,'tp'=4] {'sp'}, dimensions={0}, use_global_device_ids=true | all-gather | bytes 30720 | tf_op jit(solution)/shard_map/all_gather | solution.py:76
  30.5 19.0 %all_gather.42 = bf16[2048,128]{1,0:T(8,128)(2,1)} all-gather(bf16[512,128]{1,0:T(8,128)(2,1)S(1)} %copy-done.8), channel_id=1, replica_groups=mesh['grp'=2,'sp'=4,'tp'=4] {'sp'}, dimensions={0}, use_global_device_ids=true | all-gather | bytes 655360 | tf_op jit(solution)/shard_map/all_gather | solution.py:175
  50.2 21.1 %all_gather.41 = bf16[2048,128]{1,0:T(8,128)(2,1)} all-gather(bf16[512,128]{1,0:T(8,128)(2,1)S(1)} %copy-done.9), channel_id=1, replica_groups=mesh['grp'=2,'sp'=4,'tp'=4] {'sp'}, dimensions={0}, use_global_device_ids=true | all-gather | bytes 655360 | tf_op jit(solution)/shard_map/all_gather | solution.py:176
  74.3 2.5 multiply_reduce_fusion.1
  77.0 25.4 %all_gather.45 = bf16[1536,4,64]{0,2,1:T(8,128)(2,1)S(1)} all-gather(bf16[384,4,64]{0,2,1:T(8,128)(2,1)S(1)} %multiply_convert_fusion.2), channel_id=1, replica_groups=mesh['grp'=2,'sp'=4,'tp'=4] {'sp'}, dimensions={0}, use_global_device_ids=true | all-gather | bytes 983040 | tf_op jit(solution)/shard_map/all_gather | solution.py:115
  102.5 5.3 %all-gather.17.cloned.1.call-done = bf16[2048,256]{1,0:T(8,128)(2,1)} async-done(((bf16[512,256]{1,0:T(8,128)(2,1)}), bf16[2048,256]{1,0:T(8,128)(2,1)}) %all-gather.17.cloned.1.call-update) | async-done | bytes 1048592 | tf_op jit(solution)/shard_map/all_gather | solution.py:179
  109.7 25.2 %all_gather.47 = bf16[1536,4,64]{0,2,1:T(8,128)(2,1)S(1)} all-gather(bf16[384,4,64]{0,2,1:T(8,128)(2,1)S(1)} %bitcast.165), channel_id=1, replica_groups=mesh['grp'=2,'sp'=4,'tp'=4] {'sp'}, dimensions={0}, use_global_device_ids=true | all-gather | bytes 983040 | tf_op jit(solution)/shard_map/all_gather | solution.py:116
  134.9 8.7 %all-gather.19.cloned.1.call-done = bf16[2048,256]{1,0:T(8,128)(2,1)} async-done(((bf16[512,256]{1,0:T(8,128)(2,1)}), bf16[2048,256]{1,0:T(8,128)(2,1)}) %all-gather.19.cloned.1.call-update) | async-done | bytes 1048592 | tf_op jit(solution)/shard_map/all_gather | solution.py:177
  149.0 35.5 %conditional.1 = (f32[4,384]{1,0:T(4,128)}, f32[384,4,64]{0,2,1:T(8,128)}) conditional(s32[]{:T(128)} %bitcast.13, () %tuple.20, (bf16[1536,4,64]{0,2,1:T(8,128)(2,1)S(1)}, bf16[1536,4,64]{0,2,1:T(8,128)(2,1)S(1)}, f32[1536,4]{0,1:T(4,128)}, s32[3,512]{1,0:T(4,128)S(1)}, s32[3,512]{1,0:T(4,128)S(1)}, /*index=5*/s32[384]{0:T(512)}, ...), branch_computations={%region_7.8_spmd, %region_8.13_spmd} | conditional | flops 215199744 | bytes 15060769 | solution.py:138
  151.0 33.5 %while.18 = (s32[]{:T(128)}, f32[4,384]{1,0:T(4,128)S(1)}, f32[4,384]{1,0:T(4,128)}, f32[384,4,64]{0,2,1:T(8,128)}, s32[384]{0:T(512)}, /*index=5*/s32[3,512]{1,...) while((s32[]{:T(128)}, f32[4,384]{1,0:T(4,128)S(1)}, ...), condition=%wide.region_12.12_spmd.clone, body=%wide.region_9.11_spmd.clone.sunk | while | flops 215196672 | bytes 11896481 | solution.py:133
  153.2 2.7 fusion.85
  158.8 2.7 fusion.89
  163.8 2.7 fusion.85
  170.1 2.9 fusion.89
  175.3 2.7 fusion.85
  181.6 2.9 fusion.89
  189.8 2.8 collective-permute-start.1
  192.6 3.3 collective-permute-start
  203.8 14.9 %all-gather.23.cloned.1.call-done = bf16[2,1024,512]{2,1,0:T(8,128)(2,1)} async-done(((bf16[2,256,512]{2,1,0:T(8,128)(2,1)}), bf16[2,1024,512]{2,1,0:T(8,128)(2,1)}) %all-gather.23.cloned.1.call-update) | async-done | bytes 2097168 | tf_op jit(solution)/shard_map/all_gather | solution.py:209
  218.6 21.5 %all-gather.21.cloned.1.call-done = bf16[384,2,1024]{2,0,1:T(8,128)(2,1)} async-done(((bf16[384,2,256]{2,0,1:T(8,128)(2,1)}), bf16[384,2,1024]{2,0,1:T(8,128)(2,1)}) %all-gather.21.cloned.1.call-update) | async-done | bytes 1572880 | tf_op jit(solution)/shard_map/all_gather | solution.py:214
  240.2 3.0 convolution_bitcast_fusion
  243.2 79.3 %all-gather.11.cloned.1.call-done = bf16[2048,1024]{1,0:T(8,128)(2,1)} async-done(((bf16[512,1024]{1,0:T(8,128)(2,1)}), bf16[2048,1024]{1,0:T(8,128)(2,1)}) %all-gather.11.cloned.1.call-update) | async-done | bytes 4194320 | tf_op jit(solution)/shard_map/all_gather | solution.py:180
  322.5 5.3 %add_divide_fusion = f32[384,1024]{1,0:T(8,128)} fusion(bf16[384,2048]{1,0:T(8,128)(2,1)S(1)} %copy-done.1, bf16[2048,1024]{1,0:T(8,128)(2,1)} %all-gather.11.cloned.1.call-done), kind=kOutput, calls=%fused_computation.44 | convolution fusion | flops 1611792384 | bytes 7340032 | tf_op jit(solution)/shard_map/dot_general | solution.py:183
  327.8 2.6 reshape.258
  (143 shorter events, 51.7 us)
Async XLA Ops:
  6.5 6.6 %copy-start.15 = (f32[4,64]{1,0:T(4,128)S(1)}, f32[4,64]{1,0:T(4,128)}, u32[]{:S(2)}) copy-start(f32[4,64]{1,0:T(4,128)} %param.19) | copy-start | bytes 3076
  6.5 24.0 %copy-start.8 = (bf16[512,128]{1,0:T(8,128)(2,1)S(1)}, bf16[512,128]{1,0:T(8,128)(2,1)}, u32[]{:S(2)}) copy-start(bf16[512,128]{1,0:T(8,128)(2,1)} %param.21) | copy-start | bytes 393220
  6.5 42.9 %copy-start.16 = (f32[4]{0:T(128)S(1)}, f32[4]{0:T(128)}, u32[]{:S(2)}) copy-start(f32[4]{0:T(128)} %param.23) | copy-start | bytes 52
  6.5 43.6 %copy-start.9 = (bf16[512,128]{1,0:T(8,128)(2,1)S(1)}, bf16[512,128]{1,0:T(8,128)(2,1)}, u32[]{:S(2)}) copy-start(bf16[512,128]{1,0:T(8,128)(2,1)} %param.22) | copy-start | bytes 393220
  6.5 65.4 %all-gather.9.cloned.1.call-start = ((), (), s32[]{:S(2)}) async-start(), calls=%async_computation | async-start | bytes 1966080 | tf_op jit(solution)/shard_map/all_gather | solution.py:165
  7.3 67.1 %all-gather.15.cloned.1.call-start = ((), (), s32[]{:S(2)}) async-start(), calls=%async_computation.3 | async-start | bytes 1310720 | tf_op jit(solution)/shard_map/all_gather | solution.py:178
  8.0 99.7 %all-gather.17.cloned.1.call-start = ((), (), s32[]{:S(2)}) async-start(), calls=%async_computation.4 | async-start | bytes 1310720 | tf_op jit(solution)/shard_map/all_gather | solution.py:179
  8.8 134.9 %all-gather.19.cloned.1.call-start = ((), (), s32[]{:S(2)}) async-start(), calls=%async_computation.5 | async-start | bytes 1310720 | tf_op jit(solution)/shard_map/all_gather | solution.py:177
  9.3 176.2 %all-gather.13.cloned.1.call-start = ((), (), s32[]{:S(2)}) async-start(), calls=%async_computation.2 | async-start | bytes 1310720 | tf_op jit(solution)/shard_map/all_gather | solution.py:174
  9.9 208.7 %all-gather.23.cloned.1.call-start = ((), (), s32[]{:S(2)}) async-start(), calls=%async_computation.7 | async-start | bytes 2621440 | tf_op jit(solution)/shard_map/all_gather | solution.py:209
  10.5 63.4 %copy-start.11 = (f32[2048]{0:T(1024)S(1)}, f32[2048]{0:T(1024)}, u32[]{:S(2)}) copy-start(f32[2048]{0:T(1024)} %param.18) | copy-start | bytes 24580
  10.5 229.6 %all-gather.21.cloned.1.call-start = ((), (), s32[]{:S(2)}) async-start(), calls=%async_computation.6 | async-start | bytes 1966080 | tf_op jit(solution)/shard_map/all_gather | solution.py:214
  71.9 1.9 copy-start.2
  74.3 72.6 %copy-start = (bf16[384,2048]{1,0:T(8,128)(2,1)}, bf16[384,2048]{1,0:T(8,128)(2,1)S(1)}, u32[]{:S(2)}) copy-start(bf16[384,2048]{1,0:T(8,128)(2,1)S(1)} %fusion.27) | copy-start | bytes 4718596
  143.7 2.1 copy-start.3
  145.7 1.2 copy-start.4
  185.5 2.6 copy-start.5
  188.4 1.2 copy-start.12
  188.6 7.3 %copy-start.14 = (f32[64]{0:T(128)S(1)}, f32[64]{0:T(128)}, u32[]{:S(2)}) copy-start(f32[64]{0:T(128)} %get-tuple-element.195) | copy-start | bytes 772
  189.8 7.2 %collective-permute-start.1 = (bf16[128,2,64]{0,2,1:T(8,128)(2,1)S(1)}, bf16[128,2,64]{0,2,1:T(8,128)(2,1)S(1)}, u32[]{:S(2)}, u32[]{:S(2)}) collective-permute-start(bf16[128,2,64]{0,2,1:T(8,128)(2,1)S(1)} %slice.68), channel_id=1, source_target_pairs={{0,4},{4,8},{8,12},{1,5},{5,9},{9,13},{2,6},{6,10},{10,14},{3,7},{... | collective-permute-start | bytes 98312 | tf_op jit(solution)/shard_map/ppermute | solution.py:16
  192.6 5.4 %collective-permute-start = (bf16[128,2,64]{0,2,1:T(8,128)(2,1)S(1)}, bf16[128,2,64]{0,2,1:T(8,128)(2,1)S(1)}, u32[]{:S(2)}, u32[]{:S(2)}) collective-permute-start(bf16[128,2,64]{0,2,1:T(8,128)(2,1)S(1)} %bitcast.167), channel_id=1, source_target_pairs={{0,4},{4,8},{8,12},{1,5},{5,9},{9,13},{2,6},{6,10},{10,14},{3,7},{... | collective-permute-start | bytes 98312 | tf_op jit(solution)/shard_map/ppermute | solution.py:16
  200.9 1.5 copy-start.6
  202.4 120.1 %all-gather.11.cloned.1.call-start = ((), (), s32[]{:S(2)}) async-start(), calls=%async_computation.1 | async-start | bytes 5242880 | tf_op jit(solution)/shard_map/all_gather | solution.py:180
  203.8 118.7 %copy-start.1 = (bf16[384,2048]{1,0:T(8,128)(2,1)S(1)}, bf16[384,2048]{1,0:T(8,128)(2,1)}, u32[]{:S(2)}) copy-start(bf16[384,2048]{1,0:T(8,128)(2,1)} %copy-done) | copy-start | bytes 4718596
  (3 other events, 3.0 us)
Sparse Core Ops, SparseCore 0:
  8.9 22.3 all-gather.8
  32.9 36.9 all-gather.14
  71.5 36.1 all-gather.16
  109.1 34.4 all-gather.18
  145.1 27.0 all-gather.12
  173.6 45.0 all-gather.22
  220.2 19.9 all-gather.20
  241.7 80.7 all-gather.10
where the time goes:
time: 341 us; the launch traced here: 340 us
  waiting for transfers between devices  134 us (39%)
  blocking collectives  107 us (31%)
  matrix products  37.9 us (11%)
  other arithmetic  23.1 us (7%)
  local copies, waits for them, and re-layouts  16.3 us (5%)
  between operations  14.7 us (4%)
  starting transfers between devices  6.38 us (2%)
    all_gather x1, waiting for transfers between devices, on_device(): lax.all_gather(merge_flat, 'sp', axis=0, tiled=True)  79.3 us
    all_gather x1, blocking collectives, forget_groups(): key_rows = lax.all_gather(keys, 'sp', axis=0, tiled=True)  25.4 us
    all_gather x1, blocking collectives, forget_groups(): value_rows = lax.all_gather(values, 'sp', axis=0, tiled=True)  25.2 us
    all_gather x1, waiting for transfers between devices, on_device(): lax.all_gather(head_stack, 'tp', axis=2, tiled=True)  21.5 us
    all_gather x1, blocking collectives, on_device(): lax.all_gather(w_value_window, 'sp', axis=0, tiled=True)  21.1 us
    all_gather x1, blocking collectives, on_device(): lax.all_gather(w_key_window, 'sp', axis=0, tiled=True)  19 us
    dot_general x7, matrix products, on_device(): jnp.dot(normed, weight_rows, preferred_element_type=jnp.float32)  16.8 us
    all_gather x1, blocking collectives, forget_groups(): gates_all = lax.all_gather(gates, 'sp', axis=0, tiled=True)  16.6 us
  transfers between devices with their start and end apart: 10, of which 6 were waited for; matrix products, arithmetic and copies ran while one was open for 20% of the time, Pallas kernels for 0%

commit v1 on v0

--- a/solution.py
+++ b/solution.py
@@ -211,7 +211,7 @@
     weight_rows = branch_full
     projection = jnp.einsum(
         "uxa,xag->uxg",
-        lax.all_gather(head_stack, "tp", axis=2, tiled=True),
+        jnp.concatenate(lax.all_gather(head_stack, "tp"), axis=2),
         weight_rows,
         preferred_element_type=jnp.float32,
     )

time: 341 us -> 381 us (1.12)
  waiting for transfers between devices: 134 us -> 177 us
  local copies, waits for them, and re-layouts: 16.3 us -> 21.4 us
  other arithmetic: 23.1 us -> 18.3 us
    all_gather x1, waiting for transfers between devices: 14.9 us -> 44.4 us  [on_device(): branch_full = lax.all_gather(w_branch, 'sp', axis=1, tiled=True)]
    all_gather x1, waiting for transfers between devices: 8.71 us -> 24.1 us  [on_device(): lax.all_gather(w_query_forget, 'sp', axis=0, tiled=True)]
    all_gather x1, waiting for transfers between devices: 21.5 us -> 17.4 us  [on_device(): lax.all_gather(head_stack, 'tp')]
  transfers between devices with their start and end apart: 10 -> 10, of which waited for: 6 -> 5; matrix products, arithmetic and copies ran while one was open for 20% -> 14% of each run, Pallas kernels for 0% -> 0%
where the time goes in v1:
time: 381 us; the launch traced here: 380 us
  waiting for transfers between devices  177 us (46%)
  blocking collectives  105 us (28%)
  matrix products  36.7 us (10%)
  local copies, waits for them, and re-layouts  21.4 us (6%)
  other arithmetic  18.3 us (5%)
  between operations  14.6 us (4%)
  starting transfers between devices  7.2 us (2%)
    all_gather x1, waiting for transfers between devices, on_device(): lax.all_gather(merge_flat, 'sp', axis=0, tiled=True)  78.1 us
    all_gather x1, waiting for transfers between devices, on_device(): branch_full = lax.all_gather(w_branch, 'sp', axis=1, tiled=True)  44.4 us
    all_gather x1, blocking collectives, forget_groups(): value_rows = lax.all_gather(values, 'sp', axis=0, tiled=True)  25.3 us
    all_gather x1, blocking collectives, forget_groups(): key_rows = lax.all_gather(keys, 'sp', axis=0, tiled=True)  25 us
    all_gather x1, waiting for transfers between devices, on_device(): lax.all_gather(w_query_forget, 'sp', axis=0, tiled=True)  24.1 us
    all_gather x1, blocking collectives, on_device(): lax.all_gather(w_value_window, 'sp', axis=0, tiled=True)  22.7 us
    all_gather x1, waiting for transfers between devices, on_device(): lax.all_gather(head_stack, 'tp')  17.4 us
    all_gather x1, blocking collectives, on_device(): lax.all_gather(w_key_window, 'sp', axis=0, tiled=True)  17.2 us
  transfers between devices with their start and end apart: 10, of which 5 were waited for; matrix products, arithmetic and copies ran while one was open for 14% of the time, Pallas kernels for 0%

profile of v1, /device:TPU:0, one launch (start us, length us, event | category | flops | bytes accessed | tf_op | source)
XLA Modules:
  0.0 380.1 jit_solution(18097175595683494817)
XLA Ops:
  12.1 15.1 %all_gather.51 = f32[1536,4]{0,1:T(4,128)S(1)} all-gather(f32[384,4]{0,1:T(4,128)} %param.27), channel_id=1, replica_groups=mesh['grp'=2,'sp'=4,'tp'=4] {'sp'}, dimensions={0}, use_global_device_ids=true | all-gather | bytes 30720 | tf_op jit(solution)/shard_map/all_gather | solution.py:76
  27.3 17.2 %all_gather.45 = bf16[2048,128]{1,0:T(8,128)(2,1)} all-gather(bf16[512,128]{1,0:T(8,128)(2,1)S(1)} %copy-done.10), channel_id=1, replica_groups=mesh['grp'=2,'sp'=4,'tp'=4] {'sp'}, dimensions={0}, use_global_device_ids=true | all-gather | bytes 655360 | tf_op jit(solution)/shard_map/all_gather | solution.py:175
  44.6 22.7 %all_gather.44 = bf16[2048,128]{1,0:T(8,128)(2,1)S(1)} all-gather(bf16[512,128]{1,0:T(8,128)(2,1)S(1)} %copy-done.11), channel_id=1, replica_groups=mesh['grp'=2,'sp'=4,'tp'=4] {'sp'}, dimensions={0}, use_global_device_ids=true | all-gather | bytes 655360 | tf_op jit(solution)/shard_map/all_gather | solution.py:176
  74.5 24.1 %all-gather.20.cloned.1.call-done = bf16[2048,256]{1,0:T(8,128)(2,1)} async-done(((bf16[512,256]{1,0:T(8,128)(2,1)}), bf16[2048,256]{1,0:T(8,128)(2,1)}) %all-gather.20.cloned.1.call-update) | async-done | bytes 1048592 | tf_op jit(solution)/shard_map/all_gather | solution.py:177
  101.5 25.0 %all_gather.48 = bf16[1536,4,64]{0,2,1:T(8,128)(2,1)S(1)} all-gather(bf16[384,4,64]{0,2,1:T(8,128)(2,1)S(1)} %multiply_convert_fusion.2), channel_id=1, replica_groups=mesh['grp'=2,'sp'=4,'tp'=4] {'sp'}, dimensions={0}, use_global_device_ids=true | all-gather | bytes 983040 | tf_op jit(solution)/shard_map/all_gather | solution.py:115
  126.4 8.7 %all-gather.18.cloned.1.call-done = bf16[2048,256]{1,0:T(8,128)(2,1)} async-done(((bf16[512,256]{1,0:T(8,128)(2,1)}), bf16[2048,256]{1,0:T(8,128)(2,1)}) %all-gather.18.cloned.1.call-update) | async-done | bytes 1048592 | tf_op jit(solution)/shard_map/all_gather | solution.py:179
  137.1 25.3 %all_gather.50 = bf16[1536,4,64]{0,2,1:T(8,128)(2,1)S(1)} all-gather(bf16[384,4,64]{0,2,1:T(8,128)(2,1)S(1)} %bitcast.172), channel_id=1, replica_groups=mesh['grp'=2,'sp'=4,'tp'=4] {'sp'}, dimensions={0}, use_global_device_ids=true | all-gather | bytes 983040 | tf_op jit(solution)/shard_map/all_gather | solution.py:116
  162.4 22.7 %conditional.1 = (f32[4,384]{1,0:T(4,128)}, f32[384,4,64]{0,2,1:T(8,128)}) conditional(s32[]{:T(128)} %bitcast.13, () %tuple.20, (bf16[1536,4,64]{0,2,1:T(8,128)(2,1)S(1)}, bf16[1536,4,64]{0,2,1:T(8,128)(2,1)S(1)}, f32[1536,4]{0,1:T(4,128)S(1)}, s32[3,512]{1,0:T(4,128)S(1)}, s32[3,512]{1,0:T(4,128)S(1)}, /*index=5*/s32[384]{0:T(512)S(1)}, ...), branch_computations={%region_7.8_spmd, %region_8.13_spmd} | conditional | flops 215199744 | bytes 15060769 | solution.py:138
  163.8 21.3 %while.18 = (s32[]{:T(128)}, f32[4,384]{1,0:T(4,128)S(1)}, f32[4,384]{1,0:T(4,128)}, f32[384,4,64]{0,2,1:T(8,128)}, s32[384]{0:T(512)S(1)}, /*index=5*/s32[3,512...) while((s32[]{:T(128)}, f32[4,384]{1,0:T(4,128)S(1)}, ...), condition=%wide.region_12.12_spmd.clone, body=%wide.region_9.11_spmd.clone.sunk | while | flops 215196672 | bytes 11896481 | solution.py:133
  164.0 2.0 fusion.85
  167.6 2.7 fusion.89
  174.9 2.9 fusion.89
  182.2 2.9 fusion.89
  186.9 2.5 bitcast_reduce_fusion
  191.9 2.4 collective-permute-start.1
  195.9 4.5 %collective-permute-start = (bf16[128,2,64]{0,2,1:T(8,128)(2,1)}, bf16[128,2,64]{0,2,1:T(8,128)(2,1)S(1)}, u32[]{:S(2)}, u32[]{:S(2)}) collective-permute-start(bf16[128,2,64]{0,2,1:T(8,128)(2,1)} %bitcast.1), channel_id=1, source_target_pairs={{0,4},{4,8},{8,12},{1,5},{5,9},{9,13},{2,6},{6,10},{10,14},{3,7},{... | collective-permute-start | bytes 98312 | tf_op jit(solution)/shard_map/ppermute | solution.py:16
  210.2 2.5 fusion.32
  217.2 17.4 %all-gather.24.cloned.1.call-done = bf16[1536,2,256]{2,0,1:T(8,128)(2,1)} async-done(((bf16[384,2,256]{2,0,1:T(8,128)(2,1)}), bf16[1536,2,256]{2,0,1:T(8,128)(2,1)}) %all-gather.24.cloned.1.call-update) | async-done | bytes 1572880 | tf_op jit(solution)/shard_map/all_gather | solution.py:214
  234.6 2.9 copy.75
  237.5 44.4 %all-gather.22.cloned.1.call-done = bf16[2,1024,512]{2,1,0:T(8,128)(2,1)} async-done(((bf16[2,256,512]{2,1,0:T(8,128)(2,1)}), bf16[2,1024,512]{2,1,0:T(8,128)(2,1)}) %all-gather.22.cloned.1.call-update) | async-done | bytes 2097168 | tf_op jit(solution)/shard_map/all_gather | solution.py:209
  281.9 3.0 convolution_bitcast_fusion
  284.9 78.1 %all-gather.12.cloned.1.call-done = bf16[2048,1024]{1,0:T(8,128)(2,1)} async-done(((bf16[512,1024]{1,0:T(8,128)(2,1)}), bf16[2048,1024]{1,0:T(8,128)(2,1)}) %all-gather.12.cloned.1.call-update) | async-done | bytes 4194320 | tf_op jit(solution)/shard_map/all_gather | solution.py:180
  363.0 5.3 %add_divide_fusion = f32[384,1024]{1,0:T(8,128)} fusion(bf16[384,2048]{1,0:T(8,128)(2,1)S(1)} %copy-done.1, bf16[2048,1024]{1,0:T(8,128)(2,1)} %all-gather.12.cloned.1.call-done), kind=kOutput, calls=%fused_computation.44 | convolution fusion | flops 1611792384 | bytes 7340032 | tf_op jit(solution)/shard_map/dot_general | solution.py:183
  368.3 2.6 reshape.264
  (140 shorter events, 51.2 us)
Async XLA Ops:
  6.5 20.8 %copy-start.10 = (bf16[512,128]{1,0:T(8,128)(2,1)S(1)}, bf16[512,128]{1,0:T(8,128)(2,1)}, u32[]{:S(2)}) copy-start(bf16[512,128]{1,0:T(8,128)(2,1)} %param.21) | copy-start | bytes 393220
  6.5 37.9 %copy-start.14 = (f32[4]{0:T(128)S(1)}, f32[4]{0:T(128)}, u32[]{:S(2)}) copy-start(f32[4]{0:T(128)} %param.23) | copy-start | bytes 52
  6.5 38.0 %copy-start.11 = (bf16[512,128]{1,0:T(8,128)(2,1)S(1)}, bf16[512,128]{1,0:T(8,128)(2,1)}, u32[]{:S(2)}) copy-start(bf16[512,128]{1,0:T(8,128)(2,1)} %param.22) | copy-start | bytes 393220
  6.5 61.4 %all-gather.10.cloned.1.call-start = ((), (), s32[]{:S(2)}) async-start(), calls=%async_computation | async-start | bytes 1966080 | tf_op jit(solution)/shard_map/all_gather | solution.py:165
  7.3 65.2 %all-gather.16.cloned.1.call-start = ((), (), s32[]{:S(2)}) async-start(), calls=%async_computation.3 | async-start | bytes 1310720 | tf_op jit(solution)/shard_map/all_gather | solution.py:178
  8.0 90.6 %all-gather.20.cloned.1.call-start = ((), (), s32[]{:S(2)}) async-start(), calls=%async_computation.5 | async-start | bytes 1310720 | tf_op jit(solution)/shard_map/all_gather | solution.py:177
  8.7 126.4 %all-gather.18.cloned.1.call-start = ((), (), s32[]{:S(2)}) async-start(), calls=%async_computation.4 | async-start | bytes 1310720 | tf_op jit(solution)/shard_map/all_gather | solution.py:179
  9.3 177.6 %all-gather.14.cloned.1.call-start = ((), (), s32[]{:S(2)}) async-start(), calls=%async_computation.2 | async-start | bytes 1310720 | tf_op jit(solution)/shard_map/all_gather | solution.py:174
  9.9 60.0 %copy-start.13 = (f32[2048]{0:T(1024)S(1)}, f32[2048]{0:T(1024)}, u32[]{:S(2)}) copy-start(f32[2048]{0:T(1024)} %param.18) | copy-start | bytes 24580
  9.9 224.7 %all-gather.24.cloned.1.call-start = ((), (), s32[]{:S(2)}) async-start(), calls=%async_computation.7 | async-start | bytes 1966080 | tf_op jit(solution)/shard_map/all_gather | solution.py:214
  67.9 1.9 copy-start.2
  70.3 64.8 %copy-start = (bf16[384,2048]{1,0:T(8,128)(2,1)}, bf16[384,2048]{1,0:T(8,128)(2,1)S(1)}, u32[]{:S(2)}) copy-start(bf16[384,2048]{1,0:T(8,128)(2,1)S(1)} %fusion.27) | copy-start | bytes 4718596
  70.9 29.7 %copy-start.4 = (bf16[384,128]{0,1:T(8,128)(2,1)}, bf16[384,128]{0,1:T(8,128)(2,1)S(1)}, u32[]{:S(2)}) copy-start(bf16[384,128]{0,1:T(8,128)(2,1)S(1)} %convolution_convert_fusion.2) | copy-start | bytes 294916
  126.4 36.0 %copy-start.9 = (f32[384,4]{0,1:T(4,128)S(1)}, f32[384,4]{0,1:T(4,128)}, u32[]{:S(2)}) copy-start(f32[384,4]{0,1:T(4,128)} %param.27) | copy-start | bytes 18436
  189.4 1.4 copy-start.1
  189.4 1.5 copy-start.3
  191.9 11.0 %collective-permute-start.1 = (bf16[128,2,64]{0,2,1:T(8,128)(2,1)S(1)}, bf16[128,2,64]{0,2,1:T(8,128)(2,1)S(1)}, u32[]{:S(2)}, u32[]{:S(2)}) collective-permute-start(bf16[128,2,64]{0,2,1:T(8,128)(2,1)S(1)} %slice.68), channel_id=1, source_target_pairs={{0,4},{4,8},{8,12},{1,5},{5,9},{9,13},{2,6},{6,10},{10,14},{3,7},{... | collective-permute-start | bytes 98312 | tf_op jit(solution)/shard_map/ppermute | solution.py:16
  195.9 10.6 %collective-permute-start = (bf16[128,2,64]{0,2,1:T(8,128)(2,1)}, bf16[128,2,64]{0,2,1:T(8,128)(2,1)S(1)}, u32[]{:S(2)}, u32[]{:S(2)}) collective-permute-start(bf16[128,2,64]{0,2,1:T(8,128)(2,1)} %bitcast.1), channel_id=1, source_target_pairs={{0,4},{4,8},{8,12},{1,5},{5,9},{9,13},{2,6},{6,10},{10,14},{3,7},{... | collective-permute-start | bytes 98312 | tf_op jit(solution)/shard_map/ppermute | solution.py:16
  205.1 1.4 copy-start.5
  207.2 2.9 copy-start.12
  210.2 4.2 %copy-start.7 = (bf16[384,1,256]{2,0,1:T(8,128)(2,1)S(1)}, bf16[384,1,256]{2,0,1:T(8,128)(2,1)}, u32[]{:S(2)}) copy-start(bf16[384,1,256]{2,0,1:T(8,128)(2,1)} %copy.61) | copy-start | bytes 589828
  212.7 3.2 copy-start.6
  215.2 66.7 %all-gather.22.cloned.1.call-start = ((), (), s32[]{:S(2)}) async-start(), calls=%async_computation.6 | async-start | bytes 2621440 | tf_op jit(solution)/shard_map/all_gather | solution.py:209
  215.9 147.1 %all-gather.12.cloned.1.call-start = ((), (), s32[]{:S(2)}) async-start(), calls=%async_computation.1 | async-start | bytes 5242880 | tf_op jit(solution)/shard_map/all_gather | solution.py:180
  (1 other events, 1.3 us)
Sparse Core Ops, SparseCore 0:
  8.9 22.3 all-gather.9
  32.8 36.4 all-gather.15
  70.9 27.7 all-gather.19
  100.1 35.0 all-gather.17
  136.6 34.3 all-gather.13
  215.3 19.2 all-gather.23
  236.2 45.6 all-gather.21
  283.4 79.5 all-gather.11
